TPU v7x, 512 devices: a whole 4x8x8 slice. The times are simulated.
512 devices in a mesh: fs: 64 (over z, y), tp: 8 (over x, core).
Axes of the slice: x: 4, y: 8, z: 8, core: 2. Of those that a mesh axis runs over, the one named last changes fastest.
Arguments:
- tokens: bfloat16 [65536, 2048], P(('fs', 'tp')), may hold values from -8 to 8
- pre_mix_gain: float32 [2048], replicated, may hold values from 0.1 to 1.9
- post_mix_gain: float32 [2048], replicated, may hold values from 0.1 to 1.9
- pre_ffn_gain: float32 [2048], replicated, may hold values from 0.1 to 1.9
- post_ffn_gain: float32 [2048], replicated, may hold values from 0.1 to 1.9
- w_branch: bfloat16 [2048, 1024], P('fs', 'tp'), may hold values from -0.125 to 0.125
- w_gelu: bfloat16 [2048, 1024], P('fs', 'tp'), may hold values from -0.125 to 0.125
- conv_weight: bfloat16 [4, 1024], P(None, 'tp'), may hold values from -3 to 3
- w_rec: bfloat16 [2, 8, 128, 128], P(None, 'tp'), may hold values from -0.5 to 0.5
- w_inp: bfloat16 [2, 8, 128, 128], P(None, 'tp'), may hold values from -0.5 to 0.5
- decay: float32 [2, 1024], P(None, 'tp'), may hold values from 3 to 10
- out_weight_t: bfloat16 [2048, 1024], P('fs', 'tp'), may hold values from -0.1875 to 0.1875
- w_gate: bfloat16 [2048, 3072], P('fs', 'tp'), may hold values from -0.125 to 0.125
- w_up: bfloat16 [2048, 3072], P('fs', 'tp'), may hold values from -0.125 to 0.125
- down_weight_t: bfloat16 [2048, 3072], P('fs', 'tp'), may hold values from -0.109375 to 0.109375
Outputs:
- layer_out: bfloat16 [65536, 2048], P(('fs', 'tp'))
All inputs are finite; a program needn't handle non-finite values.
Results may differ from a plain program's by a relative error of at most 0.014.
Values may be sent and summed in bfloat16 or wider, within the bound.
A program may use at most 64 MiB of HBM per device.

v0:
```python
import jax
import jax.numpy as jnp
from jax import lax
from jax.sharding import PartitionSpec as P

EPS = 1e-06


def in_one_piece(arrays, axis, dim, along):
    both = jnp.concatenate(arrays, axis=along)
    whole, at, finished = (lax.all_gather(both, axis, axis=dim, tiled=True), 0, [])
    for a in arrays:
        finished.append(lax.slice_in_dim(whole, at, at + a.shape[along], axis=along))
        at += a.shape[along]
    return tuple(finished)


def normed(values, gain):
    factor = lax.rsqrt(jnp.mean(values * values, axis=-1, keepdims=True) + EPS)
    return values * factor * gain


def conv_short(branch, conv_weight):
    length = branch.shape[0]
    padded = jnp.pad(branch.astype(jnp.float32), ((2, 1), (0, 0)))
    weights = conv_weight.astype(jnp.float32)
    summed = weights[0] * padded[0:length]
    for offset in range(1, 4):
        summed = summed + weights[offset] * padded[offset : offset + length]
    return summed.astype(jnp.bfloat16)


def combine(earlier, later):
    return (earlier[0] * later[0], later[0] * earlier[1] + later[1])


def recurrence(conv_out, w_rec, w_inp, decay):
    length, channels = conv_out.shape
    blocks = w_rec.shape[0]
    grouped = conv_out.reshape(length, blocks, channels // blocks)
    rate_gate = jax.nn.sigmoid(
        jnp.einsum("lnc,ncd->lnd", grouped, w_rec, preferred_element_type=jnp.float32).reshape(
            length, channels
        )
    )
    inflow = jax.nn.sigmoid(
        jnp.einsum("lnc,ncd->lnd", grouped, w_inp, preferred_element_type=jnp.float32).reshape(
            length, channels
        )
    )
    log_retain = -8.0 * rate_gate * jax.nn.softplus(-decay)
    retain = jnp.exp(log_retain)
    feed = jnp.sqrt(-jnp.expm1(2.0 * log_retain)) * inflow * conv_out.astype(jnp.float32)
    unused_decay, states = lax.associative_scan(combine, (retain, feed), axis=0)
    return states


def gathered_product(normed_rows, left_weight, right_weight):
    row_piece = lax.all_gather(normed_rows, "tp", axis=0, tiled=True)
    return jnp.concatenate(
        [
            jnp.dot(row_piece, left_weight, preferred_element_type=jnp.float32),
            jnp.dot(row_piece, right_weight, preferred_element_type=jnp.float32),
        ],
        axis=1,
    )


def summed_rows(hidden, weight_t):
    return lax.psum_scatter(
        lax.dot_general(
            hidden, weight_t, (((1,), (1,)), ((), ())), preferred_element_type=jnp.float32
        ).astype(jnp.bfloat16),
        "tp",
        scatter_dimension=0,
        tiled=True,
    ).astype(jnp.float32)


def per_device(
    tokens,
    pre_mix_gain,
    post_mix_gain,
    pre_ffn_gain,
    post_ffn_gain,
    w_branch,
    w_gelu,
    conv_weight,
    w_rec,
    w_inp,
    decay,
    out_weight_t,
    w_gate,
    w_up,
    down_weight_t,
):
    branch_all, gelu_all, out_rows = in_one_piece((w_branch, w_gelu, out_weight_t), "fs", 0, 1)
    out_whole = lax.all_gather(out_rows, "tp", axis=1, tiled=True)
    stream = tokens.astype(jnp.float32)
    normed_in = normed(stream, pre_mix_gain).astype(jnp.bfloat16)
    both_in = gathered_product(normed_in, branch_all, gelu_all)
    channels = branch_all.shape[1]
    branch_in = both_in[:, :channels].astype(jnp.bfloat16)
    gelu_in = both_in[:, channels:].astype(jnp.bfloat16)
    conv_out = conv_short(branch_in, conv_weight)
    forward = recurrence(conv_out, w_rec[0], w_inp[0], decay[0])
    backward = jnp.flip(recurrence(jnp.flip(conv_out, 0), w_rec[1], w_inp[1], decay[1]), 0)
    mixer_hidden = (jax.nn.gelu(gelu_in.astype(jnp.float32)) * (forward + backward)).astype(
        jnp.bfloat16
    )
    own_hidden = lax.all_to_all(mixer_hidden, "tp", split_axis=0, concat_axis=1, tiled=True)
    mixer_sum = lax.dot_general(
        own_hidden, out_whole, (((1,), (1,)), ((), ())), preferred_element_type=jnp.float32
    )
    residual = (stream + normed(mixer_sum, post_mix_gain)).astype(jnp.bfloat16)
    middle = residual.astype(jnp.float32)
    normed_mid = normed(middle, pre_ffn_gain).astype(jnp.bfloat16)
    gate_all, up_all, down_all = in_one_piece((w_gate, w_up, down_weight_t), "fs", 0, 1)
    both_mid = gathered_product(normed_mid, gate_all, up_all)
    hidden_units = gate_all.shape[1]
    gate_proj = both_mid[:, :hidden_units]
    up_proj = both_mid[:, hidden_units:]
    ffn_hidden = (jax.nn.silu(gate_proj) * up_proj).astype(jnp.bfloat16)
    ffn_sum = summed_rows(ffn_hidden, down_all)
    return (middle + normed(ffn_sum, post_ffn_gain)).astype(jnp.bfloat16)


def solution(mesh):
    return jax.shard_map(
        per_device,
        mesh=mesh,
        in_specs=(
            P(("fs", "tp"), None),
            P(),
            P(),
            P(),
            P(),
            P("fs", "tp"),
            P("fs", "tp"),
            P(None, "tp"),
            P(None, "tp", None, None),
            P(None, "tp", None, None),
            P(None, "tp"),
            P("fs", "tp"),
            P("fs", "tp"),
            P("fs", "tp"),
            P("fs", "tp"),
        ),
        out_specs=P(("fs", "tp"), None),
        check_vma=False,
    )
```

profile of v0, /device:TPU:8, one launch (start us, length us, event | category | flops | bytes accessed | tf_op | source)
XLA Modules:
  0.0 372.8 jit_solution(1877080650165406262)
XLA Ops:
  6.5 1.3 pad_maximum_fusion.9
  7.9 1.2 fusion.29
  9.2 2.0 fusion.31
  11.3 85.9 %all-gather.8.cloned.1.call-done = bf16[2048,384]{1,0:T(8,128)(2,1)} async-done(((bf16[32,384]{1,0:T(8,128)(2,1)}), bf16[2048,384]{1,0:T(8,128)(2,1)}) %all-gather.8.cloned.1.call-update) | async-done | bytes 1572880 | tf_op jit(solution)/shard_map/all_gather | solution.py:11
  97.2 1.9 slice.729
  99.1 1.4 pad_maximum_fusion.4
  100.6 0.7 convert_element_type.60
  101.3 0.8 fusion.75
  102.1 32.2 %all-gather.6.cloned.1.call-done = bf16[1024,2048]{1,0:T(8,128)(2,1)} async-done(((bf16[128,2048]{1,0:T(8,128)(2,1)}), bf16[1024,2048]{1,0:T(8,128)(2,1)}) %all-gather.6.cloned.1.call-update) | async-done | bytes 4194320 | tf_op jit(solution)/shard_map/all_gather | solution.py:59
  134.3 3.5 fusion.25
  143.9 0.6 slice.575
  144.5 0.6 slice.592
  145.6 0.6 slice.569
  146.2 0.6 slice.594
  146.8 0.6 slice.697
  147.4 0.6 slice.563
  148.0 0.6 slice.596
  148.6 0.6 slice.696
  149.2 0.6 slice.598
  150.3 0.6 slice.551
  151.0 0.6 slice.600
  158.4 0.6 slice.661
  159.0 0.6 slice.662
  159.6 0.6 slice.660
  160.2 0.6 slice.664
  162.5 0.6 slice.647
  163.1 0.6 slice.672
  164.2 0.6 slice.641
  164.9 0.6 slice.674
  166.0 0.6 slice.635
  166.6 0.6 slice.676
  167.8 0.6 slice.629
  168.4 0.6 slice.678
  169.6 0.6 slice.623
  170.2 0.6 slice.680
  171.9 0.6 slice.711
  173.3 0.7 fusion.96
  174.1 0.8 fusion.92
  174.9 0.7 multiply_add_fusion.18
  175.6 0.6 pad_maximum_fusion.16
  176.3 0.7 multiply_add_fusion.14
  176.9 0.7 pad_maximum_fusion.14
  177.7 0.7 fusion.71
  178.4 0.7 pad_maximum_fusion.12
  179.2 0.7 fusion.69
  179.9 0.6 pad_maximum_fusion.10
  180.6 0.8 fusion.59
  181.4 0.6 pad_maximum_fusion.7
  182.1 0.7 pad_maximum_fusion.5
  182.9 0.6 pad_maximum_fusion.2
  183.6 1.7 pad.146
  185.4 1.7 pad.145
  187.1 0.8 fusion.94
  189.8 3.6 fusion.48
  193.6 10.2 %all_to_all.19 = bf16[8,128,128]{1,2,0:T(8,128)(2,1)S(1)} all-to-all(bf16[8,128,128]{1,2,0:T(8,128)(2,1)S(1)} %copy.16), channel_id=1, replica_groups=mesh['fs'=64,'tp'=8] {'tp'}, dimensions={0} | all-to-all | bytes 524288 | tf_op jit(solution)/shard_map/all_to_all | solution.py:111
  203.9 3.8 %multiply_reduce_fusion = (f32[128]{0:T(128)S(1)}, f32[128,2048]{1,0:T(8,128)S(1)}) fusion(bf16[128,1024]{0,1:T(8,128)(2,1)S(1)} %bitcast.42, bf16[2048,1024]{1,0:T(8,128)(2,1)} %all-gather.10.cloned.1.call-done), kind=kOutput, calls=%fused_computation.51 | convolution fusion | flops 537395072 | bytes 5505536 | tf_op jit(solution)/shard_map/dot_general | solution.py:112
  208.1 1.0 fusion.35
  209.3 58.9 %all-gather.14.cloned.1.call-done = bf16[2048,1152]{1,0:T(8,128)(2,1)} async-done(((bf16[32,1152]{1,0:T(8,128)(2,1)}), bf16[2048,1152]{1,0:T(8,128)(2,1)}) %all-gather.14.cloned.1.call-update) | async-done | bytes 4718608 | tf_op jit(solution)/shard_map/all_gather | solution.py:11
  268.2 36.3 %all-gather.12.cloned.1.call-done = bf16[1024,2048]{1,0:T(8,128)(2,1)} async-done(((bf16[128,2048]{1,0:T(8,128)(2,1)}), bf16[1024,2048]{1,0:T(8,128)(2,1)}) %all-gather.12.cloned.1.call-update) | async-done | bytes 4194320 | tf_op jit(solution)/shard_map/all_gather | solution.py:59
  304.5 5.0 %fusion.3 = f32[1024,384]{1,0:T(8,128)S(1)} fusion(bf16[1024,2048]{1,0:T(8,128)(2,1)} %all-gather.12.cloned.1.call-done, bf16[2048,1152]{1,0:T(8,128)(2,1)} %all-gather.14.cloned.1.call-done), kind=kOutput, calls=%fused_computation.4 | convolution fusion | flops 1610612736 | bytes 7340032 | tf_op jit(solution)/shard_map/dot_general | solution.py:62
  309.5 9.7 %convolution_convert_fusion = bf16[1024,2048]{1,0:T(8,128)(2,1)} fusion(bf16[2048,1152]{1,0:T(8,128)(2,1)} %all-gather.14.cloned.1.call-done, f32[1024,384]{1,0:T(8,128)S(1)} %fusion.3, bf16[1024,2048]{1,0:T(8,128)(2,1)} %all-gather.12.cloned.1.call-done), kind=kOutput, calls=%fused_computation | convolution fusion | flops 3225681920 | bytes 13107200 | tf_op jit(solution)/shard_map/dot_general | solution.py:71
  319.2 43.5 %reduce-scatter.2.cloned.1.call-done = bf16[128,2048]{1,0:T(8,128)(2,1)} async-done(((bf16[1024,2048]{1,0:T(8,128)(2,1)}), bf16[128,2048]{1,0:T(8,128)(2,1)}) %reduce-scatter.2.cloned.1.call-update) | async-done | bytes 524304 | tf_op jit(solution)/shard_map/reduce_scatter | solution.py:70
  362.6 1.2 fusion.27
  363.9 2.1 fusion.36
  (291 shorter events, 22.2 us)
Async XLA Ops:
  6.5 90.6 %all-gather.8.cloned.1.call-start = ((), (), s32[]{:S(2)}) async-start(), calls=%async_computation.3 | async-start | bytes 1597440 | tf_op jit(solution)/shard_map/all_gather | solution.py:11
  7.9 126.4 %all-gather.6.cloned.1.call-start = ((), (), s32[]{:S(2)}) async-start(), calls=%async_computation.2 | async-start | bytes 4718592 | tf_op jit(solution)/shard_map/all_gather | solution.py:59
  11.2 192.6 %all-gather.10.cloned.1.call-start = ((), (), s32[]{:S(2)}) async-start(), calls=%async_computation.4 | async-start | bytes 4718592 | tf_op jit(solution)/shard_map/all_gather | solution.py:98
  99.0 39.0 %copy-start.35 = (bf16[2,1,128,128]{3,2,1,0:T(8,128)(2,1)S(1)}, bf16[2,1,128,128]{3,2,1,0:T(8,128)(2,1)}, u32[]{:S(2)}) copy-start(bf16[2,1,128,128]{3,2,1,0:T(8,128)(2,1)} %param.23) | copy-start | bytes 196612
  99.1 169.1 %all-gather.14.cloned.1.call-start = ((), (), s32[]{:S(2)}) async-start(), calls=%async_computation.6 | async-start | bytes 4792320 | tf_op jit(solution)/shard_map/all_gather | solution.py:11
  100.6 203.9 %all-gather.12.cloned.1.call-start = ((), (), s32[]{:S(2)}) async-start(), calls=%async_computation.5 | async-start | bytes 4718592 | tf_op jit(solution)/shard_map/all_gather | solution.py:59
  102.1 36.4 %copy-start.36 = (bf16[2,1,128,128]{3,2,1,0:T(8,128)(2,1)S(1)}, bf16[2,1,128,128]{3,2,1,0:T(8,128)(2,1)}, u32[]{:S(2)}) copy-start(bf16[2,1,128,128]{3,2,1,0:T(8,128)(2,1)} %param.24) | copy-start | bytes 196612
  139.0 15.6 %copy-start.2 = (f32[1024,128]{1,0:T(8,128)}, f32[1024,128]{1,0:T(8,128)S(1)}, u32[]{:S(2)}) copy-start(f32[1024,128]{1,0:T(8,128)S(1)} %fusion.21) | copy-start | bytes 1572868
  141.6 11.7 %copy-start.15 = (f32[4,128]{1,0:T(4,128)}, f32[4,128]{1,0:T(4,128)S(1)}, u32[]{:S(2)}) copy-start(f32[4,128]{1,0:T(4,128)S(1)} %get-tuple-element.38) | copy-start | bytes 6148
  141.6 11.7 %copy-start.17 = (f32[4,128]{1,0:T(4,128)}, f32[4,128]{1,0:T(4,128)S(1)}, u32[]{:S(2)}) copy-start(f32[4,128]{1,0:T(4,128)S(1)} %get-tuple-element.37) | copy-start | bytes 6148
  155.8 17.5 %copy-start.1 = (f32[1024,128]{1,0:T(8,128)}, f32[1024,128]{1,0:T(8,128)S(1)}, u32[]{:S(2)}) copy-start(f32[1024,128]{1,0:T(8,128)S(1)} %fusion.24) | copy-start | bytes 1572868
  158.4 26.9 %copy-start.16 = (f32[4,128]{1,0:T(4,128)}, f32[4,128]{1,0:T(4,128)S(1)}, u32[]{:S(2)}) copy-start(f32[4,128]{1,0:T(4,128)S(1)} %get-tuple-element.42) | copy-start | bytes 6148
  158.4 26.9 %copy-start.18 = (f32[4,128]{1,0:T(4,128)}, f32[4,128]{1,0:T(4,128)S(1)}, u32[]{:S(2)}) copy-start(f32[4,128]{1,0:T(4,128)S(1)} %get-tuple-element.41) | copy-start | bytes 6148
  171.6 13.7 %slice-start.1 = ((f32[1024,128]{1,0:T(8,128)}), f32[1,128]{1,0:T(1,128)S(1)}, s32[]{:S(2)}) async-start(f32[1024,128]{1,0:T(8,128)} %copy-done.2), calls=%async_computation.9 | async-start | bytes 1024 | tf_op jit(solution)/shard_map/slice | solution.py:54
  174.0 13.1 %copy-start.24 = (f32[2,128]{1,0:T(2,128)S(1)}, f32[2,128]{1,0:T(2,128)}, u32[]{:S(2)}) copy-start(f32[2,128]{1,0:T(2,128)} %slice.661) | copy-start | bytes 3076
  174.0 13.1 %copy-start.25 = (f32[2,128]{1,0:T(2,128)S(1)}, f32[2,128]{1,0:T(2,128)}, u32[]{:S(2)}) copy-start(f32[2,128]{1,0:T(2,128)} %slice.662) | copy-start | bytes 3076
  174.0 13.1 %copy-start.26 = (f32[2,128]{1,0:T(2,128)S(1)}, f32[2,128]{1,0:T(2,128)}, u32[]{:S(2)}) copy-start(f32[2,128]{1,0:T(2,128)} %slice.660) | copy-start | bytes 3076
  174.0 13.1 %copy-start.27 = (f32[2,128]{1,0:T(2,128)S(1)}, f32[2,128]{1,0:T(2,128)}, u32[]{:S(2)}) copy-start(f32[2,128]{1,0:T(2,128)} %slice.664) | copy-start | bytes 3076
  175.6 12.4 %copy-start.22 = (f32[3,128]{1,0:T(4,128)S(1)}, f32[3,128]{1,0:T(4,128)}, u32[]{:S(2)}) copy-start(f32[3,128]{1,0:T(4,128)} %slice.653) | copy-start | bytes 4612
  175.6 12.4 %copy-start.23 = (f32[3,128]{1,0:T(4,128)S(1)}, f32[3,128]{1,0:T(4,128)}, u32[]{:S(2)}) copy-start(f32[3,128]{1,0:T(4,128)} %slice.670) | copy-start | bytes 4612
  176.2 11.8 %copy-start.34 = (f32[1,128]{1,0:T(1,128)S(1)}, f32[1,128]{1,0:T(1,128)}, u32[]{:S(2)}) copy-start(f32[1,128]{1,0:T(1,128)} %slice.651) | copy-start | bytes 1540
  176.2 11.8 %copy-start.13 = (f32[7,128]{1,0:T(8,128)S(1)}, f32[7,128]{1,0:T(8,128)}, u32[]{:S(2)}) copy-start(f32[7,128]{1,0:T(8,128)} %slice.647) | copy-start | bytes 10756
  176.2 11.8 %copy-start.14 = (f32[7,128]{1,0:T(8,128)S(1)}, f32[7,128]{1,0:T(8,128)}, u32[]{:S(2)}) copy-start(f32[7,128]{1,0:T(8,128)} %slice.672) | copy-start | bytes 10756
  177.6 10.4 %copy-start.33 = (f32[1,128]{1,0:T(1,128)S(1)}, f32[1,128]{1,0:T(1,128)}, u32[]{:S(2)}) copy-start(f32[1,128]{1,0:T(1,128)} %slice.716) | copy-start | bytes 1540
  177.6 10.5 %copy-start.11 = (f32[15,128]{1,0:T(8,128)S(1)}, f32[15,128]{1,0:T(8,128)}, u32[]{:S(2)}) copy-start(f32[15,128]{1,0:T(8,128)} %slice.641) | copy-start | bytes 23044
  177.7 10.5 %copy-start.12 = (f32[15,128]{1,0:T(8,128)S(1)}, f32[15,128]{1,0:T(8,128)}, u32[]{:S(2)}) copy-start(f32[15,128]{1,0:T(8,128)} %slice.674) | copy-start | bytes 23044
  178.4 9.8 %copy-start.32 = (f32[1,128]{1,0:T(1,128)S(1)}, f32[1,128]{1,0:T(1,128)}, u32[]{:S(2)}) copy-start(f32[1,128]{1,0:T(1,128)} %slice.715) | copy-start | bytes 1540
  179.1 9.1 %copy-start.9 = (f32[31,128]{1,0:T(8,128)S(1)}, f32[31,128]{1,0:T(8,128)}, u32[]{:S(2)}) copy-start(f32[31,128]{1,0:T(8,128)} %slice.635) | copy-start | bytes 47620
  179.1 9.1 %copy-start.10 = (f32[31,128]{1,0:T(8,128)S(1)}, f32[31,128]{1,0:T(8,128)}, u32[]{:S(2)}) copy-start(f32[31,128]{1,0:T(8,128)} %slice.676) | copy-start | bytes 47620
  179.9 8.4 %copy-start.31 = (f32[1,128]{1,0:T(1,128)S(1)}, f32[1,128]{1,0:T(1,128)}, u32[]{:S(2)}) copy-start(f32[1,128]{1,0:T(1,128)} %slice.714) | copy-start | bytes 1540
  180.5 7.8 %copy-start.7 = (f32[63,128]{1,0:T(8,128)S(1)}, f32[63,128]{1,0:T(8,128)}, u32[]{:S(2)}) copy-start(f32[63,128]{1,0:T(8,128)} %slice.629) | copy-start | bytes 96772
  180.5 7.8 %copy-start.8 = (f32[63,128]{1,0:T(8,128)S(1)}, f32[63,128]{1,0:T(8,128)}, u32[]{:S(2)}) copy-start(f32[63,128]{1,0:T(8,128)} %slice.678) | copy-start | bytes 96772
  181.4 7.0 %copy-start.30 = (f32[1,128]{1,0:T(1,128)S(1)}, f32[1,128]{1,0:T(1,128)}, u32[]{:S(2)}) copy-start(f32[1,128]{1,0:T(1,128)} %slice.713) | copy-start | bytes 1540
  182.1 6.4 %copy-start.5 = (f32[127,128]{1,0:T(8,128)S(1)}, f32[127,128]{1,0:T(8,128)}, u32[]{:S(2)}) copy-start(f32[127,128]{1,0:T(8,128)} %slice.623) | copy-start | bytes 195076
  182.1 6.4 %copy-start.6 = (f32[127,128]{1,0:T(8,128)S(1)}, f32[127,128]{1,0:T(8,128)}, u32[]{:S(2)}) copy-start(f32[127,128]{1,0:T(8,128)} %slice.680) | copy-start | bytes 195076
  182.1 6.4 %copy-start.29 = (f32[1,128]{1,0:T(1,128)S(1)}, f32[1,128]{1,0:T(1,128)}, u32[]{:S(2)}) copy-start(f32[1,128]{1,0:T(1,128)} %slice.712) | copy-start | bytes 1540
  182.9 5.8 %copy-start.28 = (f32[1,128]{1,0:T(1,128)S(1)}, f32[1,128]{1,0:T(1,128)}, u32[]{:S(2)}) copy-start(f32[1,128]{1,0:T(1,128)} %slice.711) | copy-start | bytes 1540
  185.4 3.6 slice-start
  188.6 1.0 copy-start.3
  188.6 1.2 copy-start.4
  193.4 14.3 %copy-start = (bf16[128,2048]{1,0:T(8,128)(2,1)S(1)}, bf16[128,2048]{1,0:T(8,128)(2,1)}, u32[]{:S(2)}) copy-start(bf16[128,2048]{1,0:T(8,128)(2,1)} %param.15) | copy-start | bytes 1572868
  193.4 14.2 %copy-start.19 = (f32[2048]{0:T(1024)S(1)}, f32[2048]{0:T(1024)}, u32[]{:S(2)}) copy-start(f32[2048]{0:T(1024)} %param.17) | copy-start | bytes 24580
  193.6 14.5 %copy-start.20 = (f32[2048]{0:T(1024)S(1)}, f32[2048]{0:T(1024)}, u32[]{:S(2)}) copy-start(f32[2048]{0:T(1024)} %param.18) | copy-start | bytes 24580
  209.1 153.6 %reduce-scatter.2.cloned.1.call-start = ((), (), s32[]{:S(2)}) async-start(), calls=%async_computation.7 | async-start | bytes 4718592 | tf_op jit(solution)/shard_map/reduce_scatter | solution.py:70
  319.2 44.7 %copy-start.21 = (f32[2048]{0:T(1024)S(1)}, f32[2048]{0:T(1024)}, u32[]{:S(2)}) copy-start(f32[2048]{0:T(1024)} %param.19) | copy-start | bytes 24580
Sparse Core Ops, SparseCore 0:
  10.3 86.7 all-gather.7
  99.3 34.8 all-gather.5
  136.4 40.8 all-gather.9
  180.1 87.9 all-gather.13
  270.2 34.2 all-gather.11
  319.3 43.2 reduce-scatter.1
where the time goes:
time: 374 us; the launch traced here: 373 us
  waiting for transfers between devices  257 us (69%)
  local copies, waits for them, and re-layouts  39.3 us (11%)
  matrix products  27.3 us (7%)
  other arithmetic  23.8 us (6%)
  between operations  15 us (4%)
  blocking collectives  10.2 us (3%)
    all_gather x2, waiting for transfers between devices, in_one_piece(): lax.all_gather(both, axis, axis=dim, tiled=True)  145 us
    all_gather x2, waiting for transfers between devices, gathered_product(): row_piece = lax.all_gather(normed_rows, 'tp', axis=0, tiled=True)  68.5 us
    reduce_scatter x1, waiting for transfers between devices, summed_rows(): lax.psum_scatter(lax.dot_general(hidden, weight_t, (((1,), (1,)), ((), ()...  43.5 us
    slice x122, local copies, waits for them, and re-layouts, recurrence(): unused_decay, states = lax.associative_scan(combine, (retain, feed), axis=0)  32.3 us
    all_to_all x1, blocking collectives, per_device(): lax.all_to_all(mixer_hidden, 'tp', split_axis=0, concat_axis=1, tiled=True)  10.2 us
    dot_general x1, matrix products, summed_rows(): lax.dot_general(hidden, weight_t, (((1,), (1,)), ((), ())), preferred_ele...  9.7 us
    dot_general x2, matrix products, gathered_product(): jnp.dot(row_piece, left_weight, preferred_element_type=jnp.float32)  8.54 us
  transfers between devices with their start and end apart: 6, of which 5 were waited for; matrix products, arithmetic and copies ran while one was open for 19% of the time, Pallas kernels for 0%

commit v1 on v0

--- a/solution.py
+++ b/solution.py
@@ -4,6 +4,27 @@
 from jax.sharding import PartitionSpec as P
 
 EPS = 1e-06
+
+
+def ring_gather(x, axis, dim):
+    size, place, extent = (lax.axis_size(axis), lax.axis_index(axis), x.shape[dim])
+    forward = [(i, (i + 1) % size) for i in range(size)]
+    left = [(i, (i - 1) % size) for i in range(size)]
+    filled = jnp.zeros((*x.shape[:dim], size * extent, *x.shape[dim + 1 :]), x.dtype)
+    filled = lax.dynamic_update_slice_in_dim(filled, x, place * extent, axis=dim)
+    from_left = from_right = x
+    half = size // 2
+    for step in range(1, half + 1):
+        from_left = lax.ppermute(from_left, axis, forward)
+        filled = lax.dynamic_update_slice_in_dim(
+            filled, from_left, (place - step) % size * extent, axis=dim
+        )
+        if step < size - half:
+            from_right = lax.ppermute(from_right, axis, left)
+            filled = lax.dynamic_update_slice_in_dim(
+                filled, from_right, (place + step) % size * extent, axis=dim
+            )
+    return filled
 
 
 def in_one_piece(arrays, axis, dim, along):
@@ -56,7 +77,7 @@
 
 
 def gathered_product(normed_rows, left_weight, right_weight):
-    row_piece = lax.all_gather(normed_rows, "tp", axis=0, tiled=True)
+    row_piece = ring_gather(normed_rows, "tp", 0)
     return jnp.concatenate(
         [
             jnp.dot(row_piece, left_weight, preferred_element_type=jnp.float32),

time: 374 us -> 353 us (0.944)
  waiting for transfers between devices: 257 us -> 189 us
  local copies, waits for them, and re-layouts: 39.3 us -> 60.2 us
  starting transfers between devices: 0.39 us -> 18.5 us
  other arithmetic: 23.8 us -> 30.1 us
    all_gather x2 -> x0, waiting for transfers between devices: 68.5 us -> none  [gathered_product(): row_piece = lax.all_gather(normed_rows, 'tp', axis=0, tiled=True)]
    ppermute x0 -> x14, waiting for transfers between devices: none -> 60.7 us  [the longest x8 60.5 us: ring_gather(): from_left = lax.ppermute(from_left, axis, forward)]
    all_gather x2, waiting for transfers between devices: 145 us -> 89.2 us  [in_one_piece(): lax.all_gather(both, axis, axis=dim, tiled=True)]
    ppermute x0 -> x14, starting transfers between devices: none -> 18.3 us  [the longest x6 18.3 us: ring_gather(): from_right = lax.ppermute(from_right, axis, left)]
    dynamic_update_slice x0 -> x14, local copies, waits for them, and re-layouts: none -> 11.9 us  [the longest x8 6.81 us: ring_gather(): lax.dynamic_update_slice_in_dim(filled, from_left, (place - step) % size...]
    dot_general x1 -> x2, matrix products: 3.57 us -> 8.8 us  [gathered_product(): jnp.dot(row_piece, right_weight, preferred_element_type=jnp.float32)]
    another operation x0 -> x2, local copies, waits for them, and re-layouts: none -> 5.03 us
    dot_general x2 -> x1, matrix products: 8.54 us -> 3.57 us  [gathered_product(): jnp.dot(row_piece, left_weight, preferred_element_type=jnp.float32)]
  transfers between devices with their start and end apart: 6 -> 18, of which waited for: 5 -> 11; matrix products, arithmetic and copies ran while one was open for 19% -> 28% of each run, Pallas kernels for 0% -> 0%
where the time goes in v1:
time: 353 us; the launch traced here: 352 us
  waiting for transfers between devices  189 us (54%)
  local copies, waits for them, and re-layouts  60.2 us (17%)
  other arithmetic  30.1 us (9%)
  matrix products  29.1 us (8%)
  starting transfers between devices  18.5 us (5%)
  between operations  14.4 us (4%)
  blocking collectives  9.92 us (3%)
    all_gather x2, waiting for transfers between devices, in_one_piece(): lax.all_gather(both, axis, axis=dim, tiled=True)  89.2 us
    ppermute x8, waiting for transfers between devices, ring_gather(): from_left = lax.ppermute(from_left, axis, forward)  60.5 us
    reduce_scatter x1, waiting for transfers between devices, summed_rows(): lax.psum_scatter(lax.dot_general(hidden, weight_t, (((1,), (1,)), ((), ()...  39.3 us
    slice x122, local copies, waits for them, and re-layouts, recurrence(): unused_decay, states = lax.associative_scan(combine, (retain, feed), axis=0)  36.4 us
    ppermute x6, starting transfers between devices, ring_gather(): from_right = lax.ppermute(from_right, axis, left)  18.3 us
    all_to_all x1, blocking collectives, per_device(): lax.all_to_all(mixer_hidden, 'tp', split_axis=0, concat_axis=1, tiled=True)  9.92 us
    dot_general x1, matrix products, summed_rows(): lax.dot_general(hidden, weight_t, (((1,), (1,)), ((), ())), preferred_ele...  9.72 us
    dot_general x2, matrix products, gathered_product(): jnp.dot(row_piece, right_weight, preferred_element_type=jnp.float32)  8.8 us
  transfers between devices with their start and end apart: 18, of which 11 were waited for; matrix products, arithmetic and copies ran while one was open for 28% of the time, Pallas kernels for 0%

profile of v1, /device:TPU:8, one launch (start us, length us, event | category | flops | bytes accessed | tf_op | source)
XLA Modules:
  0.0 351.5 jit_solution(8098987015684253964)
XLA Ops:
  6.6 1.4 pad_maximum_fusion.9
  8.1 89.2 %all-gather.4.cloned.1.call-done = bf16[2048,384]{1,0:T(8,128)(2,1)} async-done(((bf16[32,384]{1,0:T(8,128)(2,1)}), bf16[2048,384]{1,0:T(8,128)(2,1)}) %all-gather.4.cloned.1.call-update) | async-done | bytes 1572880 | tf_op jit(solution)/shard_map/all_gather | solution.py:32
  97.2 1.9 slice.729
  99.2 1.2 fusion.27
  100.4 2.5 broadcast.164.clone
  102.9 1.0 constant_dynamic-update-slice_fusion.15
  103.9 3.0 collective-permute-start.1
  106.9 6.9 %collective-permute-done = bf16[128,2048]{1,0:T(8,128)(2,1)S(1)} collective-permute-done((bf16[128,2048]{1,0:T(8,128)(2,1)S(1)}, bf16[128,2048]{1,0:T(8,128)(2,1)S(1)}, u32[]{:S(2)}, u32[]{:S(2)}) %collective-permute-start) | collective-permute-done | bytes 524320 | tf_op jit(solution)/shard_map/ppermute | solution.py:18
  114.7 3.5 %collective-permute-start.3 = (bf16[128,2048]{1,0:T(8,128)(2,1)S(1)}, bf16[128,2048]{1,0:T(8,128)(2,1)S(1)}, u32[]{:S(2)}, u32[]{:S(2)}) collective-permute-start(bf16[128,2048]{1,0:T(8,128)(2,1)S(1)} %collective-permute-done.1), channel_id=1, source_target_pairs={{0,7},{1,0},{2,1},{3,2},{4,3},{5,4},{6,5},{7,6},{8,15},{9,8},{10,9... | collective-permute-start | bytes 1572872 | tf_op jit(solution)/shard_map/ppermute | solution.py:23
  118.7 11.7 %collective-permute-done.2 = bf16[128,2048]{1,0:T(8,128)(2,1)S(1)} collective-permute-done((bf16[128,2048]{1,0:T(8,128)(2,1)S(1)}, bf16[128,2048]{1,0:T(8,128)(2,1)S(1)}, u32[]{:S(2)}, u32[]{:S(2)}) %collective-permute-start.2) | collective-permute-done | bytes 524320 | tf_op jit(solution)/shard_map/ppermute | solution.py:18
  130.4 0.8 constant_dynamic-update-slice_fusion.14
  131.3 0.9 constant_dynamic-update-slice_fusion.13
  132.1 2.9 collective-permute-start.5
  135.1 0.8 constant_dynamic-update-slice_fusion.12
  135.9 9.4 %collective-permute-done.4 = bf16[128,2048]{1,0:T(8,128)(2,1)S(1)} collective-permute-done((bf16[128,2048]{1,0:T(8,128)(2,1)S(1)}, bf16[128,2048]{1,0:T(8,128)(2,1)S(1)}, u32[]{:S(2)}, u32[]{:S(2)}) %collective-permute-start.4) | collective-permute-done | bytes 524320 | tf_op jit(solution)/shard_map/ppermute | solution.py:18
  145.4 0.9 constant_dynamic-update-slice_fusion.11
  146.2 0.8 constant_dynamic-update-slice_fusion.10
  147.0 0.8 constant_dynamic-update-slice_fusion.9
  147.9 7.3 %collective-permute-done.6 = bf16[128,2048]{1,0:T(8,128)(2,1)S(1)} collective-permute-done((bf16[128,2048]{1,0:T(8,128)(2,1)S(1)}, bf16[128,2048]{1,0:T(8,128)(2,1)S(1)}, u32[]{:S(2)}, u32[]{:S(2)}) %collective-permute-start.6) | collective-permute-done | bytes 524320 | tf_op jit(solution)/shard_map/ppermute | solution.py:18
  155.2 0.8 constant_dynamic-update-slice_fusion.8
  156.0 3.6 %fusion.23 = f32[1024,128]{1,0:T(8,128)S(1)} fusion(bf16[1024,2048]{1,0:T(8,128)(2,1)} %constant_dynamic-update-slice_fusion.8, bf16[2048,384]{1,0:T(8,128)(2,1)} %all-gather.4.cloned.1.call-done), kind=kOutput, calls=%fused_computation.38 | convolution fusion | flops 537133056 | bytes 5242880 | tf_op jit(solution)/shard_map/dot_general | solution.py:83
  176.0 0.9 slice.604
  178.5 1.1 fusion.101
  179.6 1.3 fusion.22
  182.2 1.4 slice.616
  183.5 1.0 fusion.81
  198.5 0.9 slice.617
  199.4 0.9 slice.682
  202.4 0.7 fusion.94
  205.9 0.7 fusion.71
  207.4 0.7 fusion.69
  208.8 0.8 fusion.59
  210.3 0.9 fusion.57
  212.0 1.0 fusion.55
  213.7 1.7 pad.146
  215.4 1.7 pad.145
  217.2 0.8 fusion.96
  220.2 0.7 fusion.68
  221.5 0.8 fusion.58
  223.1 0.9 fusion.56
  225.7 3.8 %fusion.48 = bf16[1024,128]{1,0:T(8,128)(2,1)S(1)} fusion(bf16[1024,2048]{1,0:T(8,128)(2,1)} %constant_dynamic-update-slice_fusion.8, bf16[2048,384]{1,0:T(8,128)(2,1)} %all-gather.4.cloned.1.call-done, f32[1024,128]{1,0:T(8,128)S(1)} %rev.9, f32[1024,128]{1,0:T(8,128)} %pad.145, f32[1024,128]{1,0:T(8,128)S(1)} %copy-done.5), kind=kOutput, calls=%fused_computation.62 | convolution fusion | flops 538705920 | bytes 6553600 | tf_op jit(solution)/shard_map/dot_general | solution.py:84
  229.8 9.9 %all_to_all.19 = bf16[8,128,128]{1,2,0:T(8,128)(2,1)S(1)} all-to-all(bf16[8,128,128]{1,2,0:T(8,128)(2,1)S(1)} %copy.16), channel_id=1, replica_groups=mesh['fs'=64,'tp'=8] {'tp'}, dimensions={0} | all-to-all | bytes 524288 | tf_op jit(solution)/shard_map/all_to_all | solution.py:132
  239.7 3.8 %multiply_reduce_fusion = (f32[128]{0:T(128)S(1)}, f32[128,2048]{1,0:T(8,128)S(1)}) fusion(bf16[128,1024]{0,1:T(8,128)(2,1)S(1)} %bitcast.42, bf16[2048,1024]{1,0:T(8,128)(2,1)} %all-gather.6.cloned.1.call-done), kind=kOutput, calls=%fused_computation.51 | convolution fusion | flops 537395072 | bytes 5505536 | tf_op jit(solution)/shard_map/dot_general | solution.py:133
  243.9 2.6 broadcast.164
  246.4 1.0 constant_dynamic-update-slice_fusion.7
  247.4 3.0 collective-permute-start.8
  250.4 6.9 %collective-permute-done.7 = bf16[128,2048]{1,0:T(8,128)(2,1)S(1)} collective-permute-done((bf16[128,2048]{1,0:T(8,128)(2,1)S(1)}, bf16[128,2048]{1,0:T(8,128)(2,1)S(1)}, u32[]{:S(2)}, u32[]{:S(2)}) %collective-permute-start.7) | collective-permute-done | bytes 524320 | tf_op jit(solution)/shard_map/ppermute | solution.py:18
  257.2 3.0 collective-permute-start.10
  260.2 6.9 %collective-permute-done.9 = bf16[128,2048]{1,0:T(8,128)(2,1)S(1)} collective-permute-done((bf16[128,2048]{1,0:T(8,128)(2,1)S(1)}, bf16[128,2048]{1,0:T(8,128)(2,1)S(1)}, u32[]{:S(2)}, u32[]{:S(2)}) %collective-permute-start.9) | collective-permute-done | bytes 524320 | tf_op jit(solution)/shard_map/ppermute | solution.py:18
  267.1 0.8 constant_dynamic-update-slice_fusion.6
  267.9 0.8 constant_dynamic-update-slice_fusion.5
  268.7 3.0 collective-permute-start.12
  271.7 0.9 constant_dynamic-update-slice_fusion.4
  272.6 4.3 %collective-permute-done.11 = bf16[128,2048]{1,0:T(8,128)(2,1)S(1)} collective-permute-done((bf16[128,2048]{1,0:T(8,128)(2,1)S(1)}, bf16[128,2048]{1,0:T(8,128)(2,1)S(1)}, u32[]{:S(2)}, u32[]{:S(2)}) %collective-permute-start.11) | collective-permute-done | bytes 524320 | tf_op jit(solution)/shard_map/ppermute | solution.py:18
  276.9 0.8 constant_dynamic-update-slice_fusion.3
  277.7 0.9 constant_dynamic-update-slice_fusion.2
  278.6 0.8 constant_dynamic-update-slice_fusion.1
  279.5 7.2 %collective-permute-done.13 = bf16[128,2048]{1,0:T(8,128)(2,1)S(1)} collective-permute-done((bf16[128,2048]{1,0:T(8,128)(2,1)S(1)}, bf16[128,2048]{1,0:T(8,128)(2,1)S(1)}, u32[]{:S(2)}, u32[]{:S(2)}) %collective-permute-start.13) | collective-permute-done | bytes 524320 | tf_op jit(solution)/shard_map/ppermute | solution.py:18
  286.7 0.9 constant_dynamic-update-slice_fusion
  287.6 5.0 %fusion.1 = f32[1024,384]{1,0:T(8,128)S(1)} fusion(bf16[1024,2048]{1,0:T(8,128)(2,1)} %constant_dynamic-update-slice_fusion, bf16[2048,1152]{1,0:T(8,128)(2,1)} %all-gather.8.cloned.1.call-done), kind=kOutput, calls=%fused_computation.2 | convolution fusion | flops 1610612736 | bytes 7340032 | tf_op jit(solution)/shard_map/dot_general | solution.py:84
  292.5 9.7 %convolution_convert_fusion = bf16[1024,2048]{1,0:T(8,128)(2,1)} fusion(bf16[2048,1152]{1,0:T(8,128)(2,1)} %all-gather.8.cloned.1.call-done, f32[1024,384]{1,0:T(8,128)S(1)} %fusion.1, bf16[1024,2048]{1,0:T(8,128)(2,1)} %constant_dynamic-update-slice_fusion), kind=kOutput, calls=%fused_computation | convolution fusion | flops 3225681920 | bytes 13107200 | tf_op jit(solution)/shard_map/dot_general | solution.py:92
  302.3 39.3 %reduce-scatter.2.cloned.1.call-done = bf16[128,2048]{1,0:T(8,128)(2,1)} async-done(((bf16[1024,2048]{1,0:T(8,128)(2,1)}), bf16[128,2048]{1,0:T(8,128)(2,1)}) %reduce-scatter.2.cloned.1.call-update) | async-done | bytes 524304 | tf_op jit(solution)/shard_map/reduce_scatter | solution.py:91
  341.6 1.2 fusion.25
  342.9 2.1 fusion.34
  (323 shorter events, 48.5 us)
Async XLA Ops:
  6.5 96.4 %copy-start = (bf16[128,2048]{1,0:T(8,128)(2,1)S(1)}, bf16[128,2048]{1,0:T(8,128)(2,1)}, u32[]{:S(2)}) copy-start(bf16[128,2048]{1,0:T(8,128)(2,1)} %param.15) | copy-start | bytes 1572868
  6.5 96.4 %copy-start.19 = (f32[2048]{0:T(1024)S(1)}, f32[2048]{0:T(1024)}, u32[]{:S(2)}) copy-start(f32[2048]{0:T(1024)} %param.16) | copy-start | bytes 24580
  6.5 107.2 %copy-start.12 = (bf16[32,384]{1,0:T(8,128)(2,1)S(1)}, bf16[32,384]{1,0:T(8,128)(2,1)}, u32[]{:S(2)}) copy-start(bf16[32,384]{1,0:T(8,128)(2,1)} %param.27) | copy-start | bytes 73732
  6.5 107.2 %copy-start.11 = (bf16[32,384]{1,0:T(8,128)(2,1)S(1)}, bf16[32,384]{1,0:T(8,128)(2,1)}, u32[]{:S(2)}) copy-start(bf16[32,384]{1,0:T(8,128)(2,1)} %param.28) | copy-start | bytes 73732
  6.5 107.2 %copy-start.10 = (bf16[32,384]{1,0:T(8,128)(2,1)S(1)}, bf16[32,384]{1,0:T(8,128)(2,1)}, u32[]{:S(2)}) copy-start(bf16[32,384]{1,0:T(8,128)(2,1)} %param.29) | copy-start | bytes 73732
  6.5 107.9 %copy-start.29 = (bf16[4,128]{1,0:T(4,128)(2,1)S(1)}, bf16[4,128]{1,0:T(4,128)(2,1)}, u32[]{:S(2)}) copy-start(bf16[4,128]{1,0:T(4,128)(2,1)} %param.22) | copy-start | bytes 3076
  6.6 111.7 %copy-start.30 = (f32[2,128]{1,0:T(2,128)S(1)}, f32[2,128]{1,0:T(2,128)}, u32[]{:S(2)}) copy-start(f32[2,128]{1,0:T(2,128)} %param.25) | copy-start | bytes 3076
  6.6 90.7 %all-gather.4.cloned.1.call-start = ((), (), s32[]{:S(2)}) async-start(), calls=%async_computation.2 | async-start | bytes 1597440 | tf_op jit(solution)/shard_map/all_gather | solution.py:32
  8.0 231.7 %all-gather.6.cloned.1.call-start = ((), (), s32[]{:S(2)}) async-start(), calls=%async_computation.3 | async-start | bytes 4718592 | tf_op jit(solution)/shard_map/all_gather | solution.py:119
  99.1 188.4 %all-gather.8.cloned.1.call-start = ((), (), s32[]{:S(2)}) async-start(), calls=%async_computation.4 | async-start | bytes 4792320 | tf_op jit(solution)/shard_map/all_gather | solution.py:32
  103.9 9.8 %collective-permute-start = (bf16[128,2048]{1,0:T(8,128)(2,1)S(1)}, bf16[128,2048]{1,0:T(8,128)(2,1)S(1)}, u32[]{:S(2)}, u32[]{:S(2)}) collective-permute-start(bf16[128,2048]{1,0:T(8,128)(2,1)S(1)} %get-tuple-element.10), channel_id=1, source_target_pairs={{0,1},{1,2},{2,3},{3,4},{4,5},{5,6},{6,7},{7,0},{8,9},{9,10},{10,1... | collective-permute-start | bytes 1572872 | tf_op jit(solution)/shard_map/ppermute | solution.py:18
  103.9 10.8 %collective-permute-start.1 = (bf16[128,2048]{1,0:T(8,128)(2,1)S(1)}, bf16[128,2048]{1,0:T(8,128)(2,1)S(1)}, u32[]{:S(2)}, u32[]{:S(2)}) collective-permute-start(bf16[128,2048]{1,0:T(8,128)(2,1)S(1)} %get-tuple-element.10), channel_id=1, source_target_pairs={{0,7},{1,0},{2,1},{3,2},{4,3},{5,4},{6,5},{7,6},{8,15},{9,8},{10,9... | collective-permute-start | bytes 1572872 | tf_op jit(solution)/shard_map/ppermute | solution.py:23
  113.7 16.7 %collective-permute-start.2 = (bf16[128,2048]{1,0:T(8,128)(2,1)S(1)}, bf16[128,2048]{1,0:T(8,128)(2,1)S(1)}, u32[]{:S(2)}, u32[]{:S(2)}) collective-permute-start(bf16[128,2048]{1,0:T(8,128)(2,1)S(1)} %collective-permute-done), channel_id=1, source_target_pairs={{0,1},{1,2},{2,3},{3,4},{4,5},{5,6},{6,7},{7,0},{8,9},{9,10},{10,1... | collective-permute-start | bytes 1572872 | tf_op jit(solution)/shard_map/ppermute | solution.py:18
  114.4 227.2 %reduce-scatter.2.cloned.1.call-start = ((), (), s32[]{:S(2)}) async-start(), calls=%async_computation.5 | async-start | bytes 4718592 | tf_op jit(solution)/shard_map/reduce_scatter | solution.py:91
  114.7 17.4 %collective-permute-start.3 = (bf16[128,2048]{1,0:T(8,128)(2,1)S(1)}, bf16[128,2048]{1,0:T(8,128)(2,1)S(1)}, u32[]{:S(2)}, u32[]{:S(2)}) collective-permute-start(bf16[128,2048]{1,0:T(8,128)(2,1)S(1)} %collective-permute-done.1), channel_id=1, source_target_pairs={{0,7},{1,0},{2,1},{3,2},{4,3},{5,4},{6,5},{7,6},{8,15},{9,8},{10,9... | collective-permute-start | bytes 1572872 | tf_op jit(solution)/shard_map/ppermute | solution.py:23
  130.4 14.9 %collective-permute-start.4 = (bf16[128,2048]{1,0:T(8,128)(2,1)S(1)}, bf16[128,2048]{1,0:T(8,128)(2,1)S(1)}, u32[]{:S(2)}, u32[]{:S(2)}) collective-permute-start(bf16[128,2048]{1,0:T(8,128)(2,1)S(1)} %collective-permute-done.2), channel_id=1, source_target_pairs={{0,1},{1,2},{2,3},{3,4},{4,5},{5,6},{6,7},{7,0},{8,9},{9,10},{10,1... | collective-permute-start | bytes 1572872 | tf_op jit(solution)/shard_map/ppermute | solution.py:18
  132.1 14.9 %collective-permute-start.5 = (bf16[128,2048]{1,0:T(8,128)(2,1)S(1)}, bf16[128,2048]{1,0:T(8,128)(2,1)S(1)}, u32[]{:S(2)}, u32[]{:S(2)}) collective-permute-start(bf16[128,2048]{1,0:T(8,128)(2,1)S(1)} %collective-permute-done.3), channel_id=1, source_target_pairs={{0,7},{1,0},{2,1},{3,2},{4,3},{5,4},{6,5},{7,6},{8,15},{9,8},{10,9... | collective-permute-start | bytes 1572872 | tf_op jit(solution)/shard_map/ppermute | solution.py:23
  145.3 9.8 %collective-permute-start.6 = (bf16[128,2048]{1,0:T(8,128)(2,1)S(1)}, bf16[128,2048]{1,0:T(8,128)(2,1)S(1)}, u32[]{:S(2)}, u32[]{:S(2)}) collective-permute-start(bf16[128,2048]{1,0:T(8,128)(2,1)S(1)} %collective-permute-done.4), channel_id=1, source_target_pairs={{0,1},{1,2},{2,3},{3,4},{4,5},{5,6},{6,7},{7,0},{8,9},{9,10},{10,1... | collective-permute-start | bytes 1572872 | tf_op jit(solution)/shard_map/ppermute | solution.py:18
  147.9 12.0 %copy-start.32 = (bf16[2,1,128,128]{3,2,1,0:T(8,128)(2,1)S(1)}, bf16[2,1,128,128]{3,2,1,0:T(8,128)(2,1)}, u32[]{:S(2)}) copy-start(bf16[2,1,128,128]{3,2,1,0:T(8,128)(2,1)} %param.23) | copy-start | bytes 196612
  156.0 4.2 %copy-start.33 = (bf16[2,1,128,128]{3,2,1,0:T(8,128)(2,1)S(1)}, bf16[2,1,128,128]{3,2,1,0:T(8,128)(2,1)}, u32[]{:S(2)}) copy-start(bf16[2,1,128,128]{3,2,1,0:T(8,128)(2,1)} %param.24) | copy-start | bytes 196612
  160.7 17.5 %copy-start.2 = (f32[1024,128]{1,0:T(8,128)}, f32[1024,128]{1,0:T(8,128)S(1)}, u32[]{:S(2)}) copy-start(f32[1024,128]{1,0:T(8,128)S(1)} %fusion.19) | copy-start | bytes 1572868
  163.4 13.6 %copy-start.15 = (f32[4,128]{1,0:T(4,128)}, f32[4,128]{1,0:T(4,128)S(1)}, u32[]{:S(2)}) copy-start(f32[4,128]{1,0:T(4,128)S(1)} %get-tuple-element.42) | copy-start | bytes 6148
  163.4 13.6 %copy-start.17 = (f32[4,128]{1,0:T(4,128)}, f32[4,128]{1,0:T(4,128)S(1)}, u32[]{:S(2)}) copy-start(f32[4,128]{1,0:T(4,128)S(1)} %get-tuple-element.41) | copy-start | bytes 6148
  180.9 20.7 %copy-start.1 = (f32[1024,128]{1,0:T(8,128)}, f32[1024,128]{1,0:T(8,128)S(1)}, u32[]{:S(2)}) copy-start(f32[1024,128]{1,0:T(8,128)S(1)} %fusion.22) | copy-start | bytes 1572868
  185.4 29.9 %copy-start.16 = (f32[4,128]{1,0:T(4,128)}, f32[4,128]{1,0:T(4,128)S(1)}, u32[]{:S(2)}) copy-start(f32[4,128]{1,0:T(4,128)S(1)} %get-tuple-element.46) | copy-start | bytes 6148
  185.4 29.9 %copy-start.18 = (f32[4,128]{1,0:T(4,128)}, f32[4,128]{1,0:T(4,128)S(1)}, u32[]{:S(2)}) copy-start(f32[4,128]{1,0:T(4,128)S(1)} %get-tuple-element.45) | copy-start | bytes 6148
  199.4 16.0 %slice-start.1 = ((f32[1024,128]{1,0:T(8,128)}), f32[1,128]{1,0:T(1,128)S(1)}, s32[]{:S(2)}) async-start(f32[1024,128]{1,0:T(8,128)} %copy-done.2), calls=%async_computation.7 | async-start | bytes 1024 | tf_op jit(solution)/shard_map/slice | solution.py:75
  202.3 14.8 %copy-start.25 = (f32[2,128]{1,0:T(2,128)S(1)}, f32[2,128]{1,0:T(2,128)}, u32[]{:S(2)}) copy-start(f32[2,128]{1,0:T(2,128)} %slice.661) | copy-start | bytes 3076
  202.3 14.8 %copy-start.26 = (f32[2,128]{1,0:T(2,128)S(1)}, f32[2,128]{1,0:T(2,128)}, u32[]{:S(2)}) copy-start(f32[2,128]{1,0:T(2,128)} %slice.662) | copy-start | bytes 3076
  202.3 14.8 %copy-start.27 = (f32[2,128]{1,0:T(2,128)S(1)}, f32[2,128]{1,0:T(2,128)}, u32[]{:S(2)}) copy-start(f32[2,128]{1,0:T(2,128)} %slice.660) | copy-start | bytes 3076
  202.3 14.8 %copy-start.28 = (f32[2,128]{1,0:T(2,128)S(1)}, f32[2,128]{1,0:T(2,128)}, u32[]{:S(2)}) copy-start(f32[2,128]{1,0:T(2,128)} %slice.664) | copy-start | bytes 3076
  203.9 14.1 %copy-start.23 = (f32[3,128]{1,0:T(4,128)S(1)}, f32[3,128]{1,0:T(4,128)}, u32[]{:S(2)}) copy-start(f32[3,128]{1,0:T(4,128)} %slice.653) | copy-start | bytes 4612
  203.9 14.1 %copy-start.24 = (f32[3,128]{1,0:T(4,128)S(1)}, f32[3,128]{1,0:T(4,128)}, u32[]{:S(2)}) copy-start(f32[3,128]{1,0:T(4,128)} %slice.670) | copy-start | bytes 4612
  204.5 14.2 %copy-start.13 = (f32[7,128]{1,0:T(8,128)S(1)}, f32[7,128]{1,0:T(8,128)}, u32[]{:S(2)}) copy-start(f32[7,128]{1,0:T(8,128)} %slice.647) | copy-start | bytes 10756
  204.5 14.2 %copy-start.14 = (f32[7,128]{1,0:T(8,128)S(1)}, f32[7,128]{1,0:T(8,128)}, u32[]{:S(2)}) copy-start(f32[7,128]{1,0:T(8,128)} %slice.672) | copy-start | bytes 10756
  205.9 13.6 %copy-start.8 = (f32[15,128]{1,0:T(8,128)S(1)}, f32[15,128]{1,0:T(8,128)}, u32[]{:S(2)}) copy-start(f32[15,128]{1,0:T(8,128)} %slice.641) | copy-start | bytes 23044
  205.9 13.6 %copy-start.9 = (f32[15,128]{1,0:T(8,128)S(1)}, f32[15,128]{1,0:T(8,128)}, u32[]{:S(2)}) copy-start(f32[15,128]{1,0:T(8,128)} %slice.674) | copy-start | bytes 23044
  208.1 12.1 %copy-start.7 = (f32[31,128]{1,0:T(8,128)S(1)}, f32[31,128]{1,0:T(8,128)}, u32[]{:S(2)}) copy-start(f32[31,128]{1,0:T(8,128)} %slice.635) | copy-start | bytes 47620
  210.3 12.8 %copy-start.6 = (f32[127,128]{1,0:T(8,128)S(1)}, f32[127,128]{1,0:T(8,128)}, u32[]{:S(2)}) copy-start(f32[127,128]{1,0:T(8,128)} %slice.623) | copy-start | bytes 195076
  212.0 12.7 %copy-start.3 = (f32[255,128]{1,0:T(8,128)S(1)}, f32[255,128]{1,0:T(8,128)}, u32[]{:S(2)}) copy-start(f32[255,128]{1,0:T(8,128)} %slice.617) | copy-start | bytes 391684
  212.0 12.7 %copy-start.4 = (f32[255,128]{1,0:T(8,128)S(1)}, f32[255,128]{1,0:T(8,128)}, u32[]{:S(2)}) copy-start(f32[255,128]{1,0:T(8,128)} %slice.682) | copy-start | bytes 391684
  212.9 11.8 %copy-start.31 = (f32[1,128]{1,0:T(1,128)S(1)}, f32[1,128]{1,0:T(1,128)}, u32[]{:S(2)}) copy-start(f32[1,128]{1,0:T(1,128)} %slice.711) | copy-start | bytes 1540
  215.4 9.6 %slice-start = ((f32[1024,128]{1,0:T(8,128)}), f32[1,128]{1,0:T(1,128)S(1)}, s32[]{:S(2)}) async-start(f32[1024,128]{1,0:T(8,128)} %copy-done.1), calls=%async_computation.6 | async-start | bytes 1024 | tf_op jit(solution)/shard_map/slice | solution.py:75
  224.7 1.0 copy-start.5
  229.6 13.9 %copy-start.20 = (f32[2048]{0:T(1024)S(1)}, f32[2048]{0:T(1024)}, u32[]{:S(2)}) copy-start(f32[2048]{0:T(1024)} %param.17) | copy-start | bytes 24580
  243.4 3.0 copy-start.21
  247.4 9.8 %collective-permute-start.7 = (bf16[128,2048]{1,0:T(8,128)(2,1)S(1)}, bf16[128,2048]{1,0:T(8,128)(2,1)S(1)}, u32[]{:S(2)}, u32[]{:S(2)}) collective-permute-start(bf16[128,2048]{1,0:T(8,128)(2,1)S(1)} %get-tuple-element.6), channel_id=1, source_target_pairs={{0,1},{1,2},{2,3},{3,4},{4,5},{5,6},{6,7},{7,0},{8,9},{9,10},{10,1... | collective-permute-start | bytes 1572872 | tf_op jit(solution)/shard_map/ppermute | solution.py:18
  247.4 9.8 %collective-permute-start.8 = (bf16[128,2048]{1,0:T(8,128)(2,1)S(1)}, bf16[128,2048]{1,0:T(8,128)(2,1)S(1)}, u32[]{:S(2)}, u32[]{:S(2)}) collective-permute-start(bf16[128,2048]{1,0:T(8,128)(2,1)S(1)} %get-tuple-element.6), channel_id=1, source_target_pairs={{0,7},{1,0},{2,1},{3,2},{4,3},{5,4},{6,5},{7,6},{8,15},{9,8},{10,9... | collective-permute-start | bytes 1572872 | tf_op jit(solution)/shard_map/ppermute | solution.py:23
  257.2 9.8 %collective-permute-start.9 = (bf16[128,2048]{1,0:T(8,128)(2,1)S(1)}, bf16[128,2048]{1,0:T(8,128)(2,1)S(1)}, u32[]{:S(2)}, u32[]{:S(2)}) collective-permute-start(bf16[128,2048]{1,0:T(8,128)(2,1)S(1)} %collective-permute-done.7), channel_id=1, source_target_pairs={{0,1},{1,2},{2,3},{3,4},{4,5},{5,6},{6,7},{7,0},{8,9},{9,10},{10,1... | collective-permute-start | bytes 1572872 | tf_op jit(solution)/shard_map/ppermute | solution.py:18
  257.2 11.5 %collective-permute-start.10 = (bf16[128,2048]{1,0:T(8,128)(2,1)S(1)}, bf16[128,2048]{1,0:T(8,128)(2,1)S(1)}, u32[]{:S(2)}, u32[]{:S(2)}) collective-permute-start(bf16[128,2048]{1,0:T(8,128)(2,1)S(1)} %collective-permute-done.8), channel_id=1, source_target_pairs={{0,7},{1,0},{2,1},{3,2},{4,3},{5,4},{6,5},{7,6},{8,15},{9,8},{10,9... | collective-permute-start | bytes 1572872 | tf_op jit(solution)/shard_map/ppermute | solution.py:23
  267.0 9.8 %collective-permute-start.11 = (bf16[128,2048]{1,0:T(8,128)(2,1)S(1)}, bf16[128,2048]{1,0:T(8,128)(2,1)S(1)}, u32[]{:S(2)}, u32[]{:S(2)}) collective-permute-start(bf16[128,2048]{1,0:T(8,128)(2,1)S(1)} %collective-permute-done.9), channel_id=1, source_target_pairs={{0,1},{1,2},{2,3},{3,4},{4,5},{5,6},{6,7},{7,0},{8,9},{9,10},{10,1... | collective-permute-start | bytes 1572872 | tf_op jit(solution)/shard_map/ppermute | solution.py:18
  268.7 9.9 %collective-permute-start.12 = (bf16[128,2048]{1,0:T(8,128)(2,1)S(1)}, bf16[128,2048]{1,0:T(8,128)(2,1)S(1)}, u32[]{:S(2)}, u32[]{:S(2)}) collective-permute-start(bf16[128,2048]{1,0:T(8,128)(2,1)S(1)} %collective-permute-done.10), channel_id=1, source_target_pairs={{0,7},{1,0},{2,1},{3,2},{4,3},{5,4},{6,5},{7,6},{8,15},{9,8},{10,9... | collective-permute-start | bytes 1572872 | tf_op jit(solution)/shard_map/ppermute | solution.py:23
  276.9 9.8 %collective-permute-start.13 = (bf16[128,2048]{1,0:T(8,128)(2,1)S(1)}, bf16[128,2048]{1,0:T(8,128)(2,1)S(1)}, u32[]{:S(2)}, u32[]{:S(2)}) collective-permute-start(bf16[128,2048]{1,0:T(8,128)(2,1)S(1)} %collective-permute-done.11), channel_id=1, source_target_pairs={{0,1},{1,2},{2,3},{3,4},{4,5},{5,6},{6,7},{7,0},{8,9},{9,10},{10,1... | collective-permute-start | bytes 1572872 | tf_op jit(solution)/shard_map/ppermute | solution.py:18
  302.3 40.6 %copy-start.22 = (f32[2048]{0:T(1024)S(1)}, f32[2048]{0:T(1024)}, u32[]{:S(2)}) copy-start(f32[2048]{0:T(1024)} %param.19) | copy-start | bytes 24580
Sparse Core Ops, SparseCore 0:
  10.4 86.7 all-gather.3
  99.3 45.7 all-gather.5
  148.1 89.4 all-gather.7
  302.4 39.1 reduce-scatter.1
